TPU v7x, 32 devices: a whole 2x2x4 slice. The times are simulated.
32 devices in a mesh: rep: 4 (over z), fs: 2 (over y), tp: 4 (over x, core).
Axes of the slice: x: 2, y: 2, z: 4, core: 2. Of those that a mesh axis runs over, the one named last changes fastest.
Arguments:
- tokens: bfloat16 [3072, 2048], P('rep', 'fs'), may hold values from -6 to 6
- gate_pre: bfloat16 [3072, 6144], P('rep', 'tp'), may hold values from -6 to 6
- up_pre: bfloat16 [3072, 6144], P('rep', 'tp'), may hold values from -6 to 6
- hidden_grad: bfloat16 [3072, 6144], P('rep', 'tp'), may hold values from -0.75 to 0.75
- gate_weight: bfloat16 [2048, 6144], P('fs', 'tp'), may hold values from -0.125 to 0.125
- up_weight: bfloat16 [2048, 6144], P('fs', 'tp'), may hold values from -0.125 to 0.125
- gate_taps: float32 [3, 6144], P(None, 'tp'), may hold values from -3.5 to 3.5
- up_taps: float32 [3, 6144], P(None, 'tp'), may hold values from -3.5 to 3.5
- gate_bias: float32 [6144], P('tp'), may hold values from -4 to 4
- up_bias: float32 [6144], P('tp'), may hold values from -4 to 4
Outputs:
- input_grad: bfloat16 [3072, 2048], P('rep', 'fs')
- gate_weight_grad: float32 [2048, 6144], P('fs', 'tp')
- up_weight_grad: float32 [2048, 6144], P('fs', 'tp')
- gate_taps_grad: float32 [3, 6144], P(None, 'tp')
- up_taps_grad: float32 [3, 6144], P(None, 'tp')
- gate_bias_grad: float32 [6144], P('tp')
- up_bias_grad: float32 [6144], P('tp')
All inputs are finite; a program needn't handle non-finite values.
Results may differ from a plain program's by a relative error of at most 0.017.
Values may be sent and summed in bfloat16 or wider, within the bound.
A program may use at most 64 MiB of HBM per device.

v0:
```python
import functools

import jax
import jax.numpy as jnp
from jax import lax
from jax.experimental import pallas as pl
from jax.experimental.pallas import tpu as pltpu
from jax.sharding import PartitionSpec as P

MESH = pl.DeviceIdType.MESH
CW = 128
NQ = 8
PAD = 8
F32 = jnp.float32
BF16 = jnp.bfloat16


def schedule(blocks, rep_count):
    warm = min(3, blocks)
    done = warm + (blocks - warm + 1) // 2
    steps = max(blocks + rep_count - 1, done + rep_count, done + 3)
    return warm, done, steps


def fused(
    rep_count,
    tp_count,
    tokens,
    gate_pre,
    up_pre,
    hidden,
    gate_weight,
    up_weight,
    gate_taps,
    up_taps,
    gate_bias,
    up_bias,
    grad_out,
    gate_out,
    up_out,
    small_out,
    tok,
    tok_t,
    gpre,
    upre,
    hid,
    gw,
    uw,
    gpad,
    upad,
    gdel,
    udel,
    back,
    acc,
    own,
    from_left,
    from_right,
    to_right,
    to_left,
    out_stage,
    term,
    term_in,
    final,
    small,
    small_from_left,
    small_from_right,
    small_to_right,
    small_to_left,
    load_sem,
    weight_sem,
    send_r,
    recv_r,
    send_l,
    recv_l,
    out_sem,
    scatter_send,
    scatter_recv,
    gather_send,
    gather_recv,
    final_sem,
    small_sem,
):
    z = lax.axis_index("rep")
    me = lax.axis_index("tp")
    length, hidden_cols = gate_pre.shape
    width = tokens.shape[1]
    blocks = hidden_cols // CW
    rows_q = width // NQ
    taps = gate_taps.shape[0]
    warm, done, steps = schedule(blocks, rep_count)
    has_left = z > 0
    has_right = z < rep_count - 1

    def columns(b):
        return pl.ds(pl.multiple_of(b * CW, CW), CW)

    def load(which, b):
        src = (gate_pre, up_pre, hidden)[which]
        dst = (gpre, upre, hid)[which]
        return pltpu.make_async_copy(
            src.at[:, columns(b)], dst.at[b], load_sem.at[which, b]
        )

    token_copy = pltpu.make_async_copy(tokens, tok, weight_sem.at[0])
    weight_copies = (
        pltpu.make_async_copy(gate_weight, gw, weight_sem.at[1]),
        pltpu.make_async_copy(up_weight, uw, weight_sem.at[2]),
    )
    for which in range(3):
        load(which, 0).start()
    token_copy.start()

    def start_load(b, carry):
        for which in range(3):
            load(which, b).start()
        return carry

    lax.fori_loop(1, blocks, start_load, 0)
    for copy in weight_copies:
        copy.start()

    barrier = pltpu.get_barrier_semaphore()

    @pl.when(has_left)
    def _():
        pl.semaphore_signal(barrier, inc=1, device_id={"rep": z - 1}, device_id_type=MESH)

    @pl.when(has_right)
    def _():
        pl.semaphore_signal(barrier, inc=1, device_id={"rep": z + 1}, device_id_type=MESH)

    for d in range(1, tp_count):
        peer = lax.rem(me + d, tp_count)
        pl.semaphore_signal(barrier, inc=1, device_id={"tp": peer}, device_id_type=MESH)

    @pl.when(z == 0)
    def _():
        small_from_left[...] = jnp.zeros_like(small_from_left)

        def clear(c, carry):
            from_left[c] = jnp.zeros((rows_q, 2 * CW), BF16)
            return carry

        lax.fori_loop(0, blocks * NQ, clear, 0)

    @pl.when(z == rep_count - 1)
    def _():
        small_from_right[...] = jnp.zeros_like(small_from_right)

        def clear(c, carry):
            from_right[c] = jnp.zeros((rows_q, 2 * CW), BF16)
            return carry

        lax.fori_loop(0, blocks * NQ, clear, 0)

    zero_rows = jnp.zeros((PAD, CW), F32)
    gpad[0:PAD, :] = zero_rows
    upad[0:PAD, :] = zero_rows
    gdel[length : length + PAD, :] = zero_rows
    udel[length : length + PAD, :] = zero_rows
    acc[...] = jnp.zeros_like(acc)

    token_copy.wait()
    for i in range(width // CW):
        tok_t[i * CW : (i + 1) * CW, :] = tok[:, i * CW : (i + 1) * CW].T

    pl.semaphore_wait(
        barrier,
        jnp.where(has_left, 1, 0) + jnp.where(has_right, 1, 0) + (tp_count - 1),
    )

    row_tile = 128 if length % 128 == 0 else length

    def folded(x):
        return jnp.sum(x.reshape(x.shape[0] // 8, 8, CW), axis=0)

    def compute(b, carry):
        for which in range(3):
            load(which, b).wait()
        cols = columns(b)
        gt = [gate_taps[k : k + 1, cols] for k in range(taps)]
        ut = [up_taps[k : k + 1, cols] for k in range(taps)]
        gb = gate_bias[cols].reshape(1, CW)
        ub = up_bias[cols].reshape(1, CW)
        for r in range(0, length, row_tile):
            gpad[PAD + r : PAD + r + row_tile, :] = gpre[b, r : r + row_tile, :].astype(F32)
            upad[PAD + r : PAD + r + row_tile, :] = upre[b, r : r + row_tile, :].astype(F32)
        sums = None
        for r in range(0, length, row_tile):
            start = PAD + r - (taps - 1)
            gs = [gpad[start + k : start + k + row_tile, :] for k in range(taps)]
            us = [upad[start + k : start + k + row_tile, :] for k in range(taps)]
            gm = gs[0] * gt[0]
            um = us[0] * ut[0]
            for k in range(1, taps):
                gm = gm + gs[k] * gt[k]
                um = um + us[k] * ut[k]
            gm = gm + gb
            um = um + ub
            s = jax.nn.sigmoid(gm)
            h = hid[b, r : r + row_tile, :].astype(F32)
            gd = h * um * s * (1.0 + gm * (1.0 - s))
            ud = h * gm * s
            gdel[r : r + row_tile, :] = gd
            udel[r : r + row_tile, :] = ud
            parts = (
                [folded(gd * g) for g in gs]
                + [folded(ud * u) for u in us]
                + [folded(gd), folded(ud)]
            )
            sums = parts if sums is None else [a + p for a, p in zip(sums, parts)]
        for k, part in enumerate(sums):
            small[k : k + 1, cols] = jnp.sum(part, axis=0, keepdims=True)
        for r in range(0, length, row_tile):
            first = r + taps - 1
            gk = gdel[first : first + row_tile, :] * gt[0]
            uk = udel[first : first + row_tile, :] * ut[0]
            for k in range(1, taps):
                first = r + taps - 1 - k
                gk = gk + gdel[first : first + row_tile, :] * gt[k]
                uk = uk + udel[first : first + row_tile, :] * ut[k]
            back[r : r + row_tile, 0:CW] = gk.astype(BF16)
            back[r : r + row_tile, CW : 2 * CW] = uk.astype(BF16)
        block = back[...]
        for q in range(NQ):
            own[b * NQ + q] = jnp.dot(
                tok_t[q * rows_q : (q + 1) * rows_q, :], block, preferred_element_type=F32
            ).astype(BF16)

        @pl.when(b == 0)
        def _():
            for copy in weight_copies:
                copy.wait()

        weights = jnp.concatenate([gw[:, cols], uw[:, cols]], axis=1)
        dot_rows = 256 if length % 256 == 0 else length
        for r in range(0, length, dot_rows):
            acc[r : r + dot_rows, :] += lax.dot_general(
                back[r : r + dot_rows, :],
                weights,
                (((1,), (1,)), ((), ())),
                preferred_element_type=F32,
            )
        return carry

    def right_copy(c):
        return pltpu.make_async_remote_copy(
            src_ref=to_right.at[c],
            dst_ref=from_left.at[c],
            send_sem=send_r.at[c],
            recv_sem=recv_r.at[c],
            device_id={"rep": z + 1},
            device_id_type=MESH,
        )

    def left_copy(c):
        return pltpu.make_async_remote_copy(
            src_ref=to_left.at[c],
            dst_ref=from_right.at[c],
            send_sem=send_l.at[c],
            recv_sem=recv_l.at[c],
            device_id={"rep": z - 1},
            device_id_type=MESH,
        )

    small_right = pltpu.make_async_remote_copy(
        src_ref=small_to_right,
        dst_ref=small_from_left,
        send_sem=small_sem.at[0],
        recv_sem=small_sem.at[1],
        device_id={"rep": z + 1},
        device_id_type=MESH,
    )
    small_left = pltpu.make_async_remote_copy(
        src_ref=small_to_left,
        dst_ref=small_from_right,
        send_sem=small_sem.at[2],
        recv_sem=small_sem.at[3],
        device_id={"rep": z - 1},
        device_id_type=MESH,
    )

    def out_copies(b, q):
        rows = pl.ds(q * rows_q, rows_q)
        return (
            pltpu.make_async_copy(
                out_stage.at[0, q], gate_out.at[rows, columns(b)], out_sem.at[0, q]
            ),
            pltpu.make_async_copy(
                out_stage.at[1, q], up_out.at[rows, columns(b)], out_sem.at[1, q]
            ),
        )

    def scatter_copy(d):
        peer = lax.rem(me + d, tp_count)
        return pltpu.make_async_remote_copy(
            src_ref=term.at[peer],
            dst_ref=term_in.at[d - 1],
            send_sem=scatter_send.at[d - 1],
            recv_sem=scatter_recv.at[d - 1],
            device_id={"tp": peer},
            device_id_type=MESH,
        )

    def gather_copy(d, slot):
        return pltpu.make_async_remote_copy(
            src_ref=final.at[slot],
            dst_ref=final.at[slot],
            send_sem=gather_send.at[d - 1],
            recv_sem=gather_recv.at[d - 1],
            device_id={"tp": lax.rem(me + d, tp_count)},
            device_id_type=MESH,
        )

    term_rows = length // tp_count

    def step(s, carry):
        first = jnp.where(s < warm, s, 2 * s - warm)
        last = jnp.minimum(jnp.where(s < warm, s + 1, 2 * s - warm + 2), blocks)
        lax.fori_loop(first, last, compute, 0)

        b_right = s - z
        b_left = s - (rep_count - 1 - z)
        b_out = s - (rep_count - 1)
        for q in range(NQ):

            @pl.when((b_right >= 0) & (b_right < blocks))
            def _():
                c = b_right * NQ + q

                @pl.when(has_left)
                def _():
                    right_copy(c).wait_recv()

                @pl.when(has_right)
                def _():
                    to_right[c] = (from_left[c].astype(F32) + own[c].astype(F32)).astype(BF16)
                    right_copy(c).start()

            @pl.when((b_left >= 0) & (b_left < blocks))
            def _():
                c = b_left * NQ + q

                @pl.when(has_right)
                def _():
                    left_copy(c).wait_recv()

                @pl.when(has_left)
                def _():
                    to_left[c] = (from_right[c].astype(F32) + own[c].astype(F32)).astype(BF16)
                    left_copy(c).start()

            @pl.when((b_out >= 0) & (b_out < blocks))
            def _():
                c = b_out * NQ + q

                @pl.when(b_out > 0)
                def _():
                    for copy in out_copies(b_out - 1, q):
                        copy.wait()

                total = (
                    from_left[c].astype(F32) + own[c].astype(F32) + from_right[c].astype(F32)
                ).astype(BF16)
                out_stage[0, q] = total[:, 0:CW]
                out_stage[1, q] = total[:, CW : 2 * CW]
                for copy in out_copies(b_out, q):
                    copy.start()

        @pl.when(s == done)
        def _():
            for k in range(tp_count):
                term[k] = acc[k * term_rows : (k + 1) * term_rows, :].astype(BF16)
            for d in range(1, tp_count):
                scatter_copy(d).start()

        @pl.when(s == done + 2)
        def _():
            total = term[me].astype(F32)
            for d in range(1, tp_count):
                scatter_copy(d).wait()
                total = total + term_in[d - 1].astype(F32)
            final[me] = total.astype(BF16)
            for d in range(1, tp_count):
                gather_copy(d, me).start()

        @pl.when(s == done + z)
        def _():
            @pl.when(has_left)
            def _():
                small_right.wait_recv()

            @pl.when(has_right)
            def _():
                small_to_right[...] = small_from_left[...] + small[...]
                small_right.start()

        @pl.when(s == done + rep_count - 1 - z)
        def _():
            @pl.when(has_right)
            def _():
                small_left.wait_recv()

            @pl.when(has_left)
            def _():
                small_to_left[...] = small_from_right[...] + small[...]
                small_left.start()

        return carry

    lax.fori_loop(0, steps, step, 0)

    def final_copy(slot):
        return pltpu.make_async_copy(
            final.at[slot],
            grad_out.at[pl.ds(pl.multiple_of(slot * term_rows, term_rows), term_rows), :],
            final_sem.at[slot],
        )

    final_copy(me).start()
    for d in range(1, tp_count):
        sender = lax.rem(me + tp_count - d, tp_count)
        gather_copy(d, sender).wait_recv()
        final_copy(sender).start()
    for d in range(1, tp_count):
        gather_copy(d, me).wait_send()
    small_out[...] = small_from_left[...] + small[...] + small_from_right[...]

    @pl.when(has_right)
    def _():
        small_right.wait_send()

        def drain(c, carry):
            right_copy(c).wait_send()
            return carry

        lax.fori_loop(0, blocks * NQ, drain, 0)

    @pl.when(has_left)
    def _():
        small_left.wait_send()

        def drain(c, carry):
            left_copy(c).wait_send()
            return carry

        lax.fori_loop(0, blocks * NQ, drain, 0)

    for q in range(NQ):
        for copy in out_copies(blocks - 1, q):
            copy.wait()
    for slot in range(tp_count):
        final_copy(slot).wait()


def per_device(
    rep_count,
    tp_count,
    tokens,
    gate_pre,
    up_pre,
    hidden_grad,
    gate_weight,
    up_weight,
    gate_taps,
    up_taps,
    gate_bias,
    up_bias,
):
    length, hidden_cols = gate_pre.shape
    width = tokens.shape[1]
    taps = gate_taps.shape[0]
    blocks = hidden_cols // CW
    chunks = blocks * NQ
    rows_q = width // NQ
    term_rows = length // tp_count
    small_rows = 2 * taps + 2
    anywhere = pl.BlockSpec(memory_space=pl.ANY)
    vmem = pl.BlockSpec(memory_space=pltpu.VMEM)
    line = pltpu.VMEM((chunks, rows_q, 2 * CW), BF16)
    small = pltpu.VMEM((small_rows, hidden_cols), F32)
    dma = pltpu.SemaphoreType.DMA
    grad, gate_sum, up_sum, small_sum = pl.pallas_call(
        functools.partial(fused, rep_count, tp_count),
        out_shape=(
            jax.ShapeDtypeStruct((length, width), BF16),
            jax.ShapeDtypeStruct((width, hidden_cols), BF16),
            jax.ShapeDtypeStruct((width, hidden_cols), BF16),
            jax.ShapeDtypeStruct((small_rows, hidden_cols), F32),
        ),
        in_specs=[anywhere] * 6 + [vmem] * 4,
        out_specs=(anywhere, anywhere, anywhere, vmem),
        scratch_shapes=[
            pltpu.VMEM((length, width), BF16),
            pltpu.VMEM((width, length), BF16),
            pltpu.VMEM((blocks, length, CW), BF16),
            pltpu.VMEM((blocks, length, CW), BF16),
            pltpu.VMEM((blocks, length, CW), BF16),
            pltpu.VMEM((width, hidden_cols), BF16),
            pltpu.VMEM((width, hidden_cols), BF16),
            pltpu.VMEM((PAD + length, CW), F32),
            pltpu.VMEM((PAD + length, CW), F32),
            pltpu.VMEM((length + PAD, CW), F32),
            pltpu.VMEM((length + PAD, CW), F32),
            pltpu.VMEM((length, 2 * CW), BF16),
            pltpu.VMEM((length, width), F32),
            line,
            line,
            line,
            line,
            line,
            pltpu.VMEM((2, NQ, rows_q, CW), BF16),
            pltpu.VMEM((tp_count, term_rows, width), BF16),
            pltpu.VMEM((tp_count - 1, term_rows, width), BF16),
            pltpu.VMEM((tp_count, term_rows, width), BF16),
            small,
            small,
            small,
            small,
            small,
            dma((3, blocks)),
            dma((3,)),
            dma((chunks,)),
            dma((chunks,)),
            dma((chunks,)),
            dma((chunks,)),
            dma((2, NQ)),
            dma((tp_count - 1,)),
            dma((tp_count - 1,)),
            dma((tp_count - 1,)),
            dma((tp_count - 1,)),
            dma((tp_count,)),
            dma((4,)),
        ],
        compiler_params=pltpu.CompilerParams(
            collective_id=0, has_side_effects=True, vmem_limit_bytes=67043328
        ),
    )(
        tokens,
        gate_pre,
        up_pre,
        hidden_grad,
        gate_weight,
        up_weight,
        gate_taps,
        up_taps,
        gate_bias,
        up_bias,
    )
    return (
        grad,
        gate_sum.astype(F32),
        up_sum.astype(F32),
        small_sum[0:taps],
        small_sum[taps : 2 * taps],
        small_sum[2 * taps],
        small_sum[2 * taps + 1],
    )


def solution(mesh):
    return jax.shard_map(
        functools.partial(per_device, mesh.shape["rep"], mesh.shape["tp"]),
        mesh=mesh,
        in_specs=(
            P("rep", "fs"),
            P("rep", "tp"),
            P("rep", "tp"),
            P("rep", "tp"),
            P("fs", "tp"),
            P("fs", "tp"),
            P(None, "tp"),
            P(None, "tp"),
            P("tp"),
            P("tp"),
        ),
        out_specs=(
            P("rep", "fs"),
            P("fs", "tp"),
            P("fs", "tp"),
            P(None, "tp"),
            P(None, "tp"),
            P("tp"),
            P("tp"),
        ),
        check_vma=False,
    )
```

profile of v0, /device:TPU:0, one launch (start us, length us, event | category | flops | bytes accessed | tf_op | source)
XLA Modules:
  0.0 180.8 jit_solution(7863464995203314822)
XLA Ops:
  0.6 168.6 %shard_map.153 = (bf16[768,1024]{1,0:T(8,128)(2,1)}, bf16[1024,1536]{1,0:T(8,128)(2,1)}, bf16[1024,1536]{1,0:T(8,128)(2,1)}, f32[8,1536]{1,0:T(8,128)}) custom-call(bf16[768,1024]{1,0:T(8,128)(2,1)} %tokens.1, bf16[768,1536]{1,0:T(8,128)(2,1)} %gate_pre.1, bf16[768,1536]{1,0:T(8,128)(2,1)} %up_pre.1, bf16[768,1536]{1,0:T(8,128)(2,1)} %hidden.1, ...), custom_call_target="tpu_custom_call" | custom-call | tf_op jit(solution)/shard_map/pallas_call | solution.py:483
  169.2 0.0 copy-start
  169.2 5.6 %convert_element_type.6 = f32[1024,1536]{1,0:T(8,128)} convert(bf16[1024,1536]{1,0:T(8,128)(2,1)} %get-tuple-element.12) | non-fusion elementwise | flops 1572864 | bytes 9437184 | tf_op jit(solution)/shard_map/convert_element_type | solution.py:552
  174.8 0.0 copy-done
  174.8 0.0 copy-start.2
  174.8 0.0 copy-start.1
  174.8 3.6 %convert_element_type.7 = f32[1024,1536]{1,0:T(8,128)} convert(bf16[1024,1536]{1,0:T(8,128)(2,1)S(1)} %copy-done) | non-fusion elementwise | flops 1572864 | bytes 9437184 | tf_op jit(solution)/shard_map/convert_element_type | solution.py:553
  178.4 0.0 copy-done.2
  178.4 0.6 fusion
  179.0 0.6 slice_reduce_fusion
  179.7 0.0 copy-done.1
  179.7 1.1 copy.18
Async XLA Ops:
  169.2 5.6 %copy-start = (bf16[1024,1536]{1,0:T(8,128)(2,1)S(1)}, bf16[1024,1536]{1,0:T(8,128)(2,1)}, u32[]{:S(2)}) copy-start(bf16[1024,1536]{1,0:T(8,128)(2,1)} %get-tuple-element.13) | copy-start | bytes 9437188
  174.8 3.6 %copy-start.2 = (f32[8,1536]{1,0:T(8,128)S(1)}, f32[8,1536]{1,0:T(8,128)}, u32[]{:S(2)}) copy-start(f32[8,1536]{1,0:T(8,128)} %get-tuple-element.14) | copy-start | bytes 147460
  174.8 4.8 %copy-start.1 = (bf16[768,1024]{1,0:T(8,128)(2,1)S(1)}, bf16[768,1024]{1,0:T(8,128)(2,1)}, u32[]{:S(2)}) copy-start(bf16[768,1024]{1,0:T(8,128)(2,1)} %get-tuple-element.26) | copy-start | bytes 4718596
where the time goes:
time: 181 us
  Pallas kernels  169 us (93%)
  other arithmetic  9.19 us (5%)
  local copies, waits for them, and re-layouts  2.41 us (1%)
    pallas_call x1, Pallas kernels, per_device(): pl.pallas_call(functools.partial(fused, rep_count, tp_count), out_shape=(...  169 us
    convert_element_type x1, other arithmetic, per_device(): gate_sum.astype(F32)  5.62 us

commit v1 on v0

v1 whole, which is shorter than its diff:
```python
import functools

import jax
import jax.numpy as jnp
from jax import lax
from jax.experimental import pallas as pl
from jax.experimental.pallas import tpu as pltpu
from jax.sharding import PartitionSpec as P

MESH = pl.DeviceIdType.MESH
CW = 128
NQ = 8
PAD = 8
TICKS = 4
LAG = 4
TILE = 32
F32 = jnp.float32
BF16 = jnp.bfloat16


def schedule(blocks, rep_count):
    done = max(blocks - 1, 0)
    last_tick = blocks * NQ + LAG * (rep_count - 1)
    steps = max(-(-last_tick // TICKS), done + rep_count, done + 5)
    return done, steps


def fused(
    rep_count,
    tp_count,
    tokens,
    gate_pre,
    up_pre,
    hidden,
    gate_weight,
    up_weight,
    gate_taps,
    up_taps,
    gate_bias,
    up_bias,
    own,
    final,
    small_out,
    tok,
    tok_t,
    gpre,
    upre,
    hid,
    gw,
    uw,
    gpad,
    upad,
    gdel,
    udel,
    gback,
    uback,
    parts_ref,
    acc,
    from_left,
    from_right,
    to_left,
    term,
    term_in,
    small,
    small_from_left,
    small_from_right,
    small_to_right,
    small_to_left,
    load_sem,
    weight_sem,
    send_r,
    recv_r,
    send_l,
    recv_l,
    scatter_send,
    scatter_recv,
    gather_send,
    gather_recv,
    small_sem,
):
    z = lax.axis_index("rep")
    me = lax.axis_index("tp")
    length, hidden_cols = gate_pre.shape
    width = tokens.shape[1]
    blocks = hidden_cols // CW
    chunks = blocks * NQ
    rows_q = width // NQ
    taps = gate_taps.shape[0]
    done, steps = schedule(blocks, rep_count)
    has_left = z > 0
    has_right = z < rep_count - 1
    both = has_left & has_right

    def columns(b):
        return pl.ds(pl.multiple_of(b * CW, CW), CW)

    def load(which, b):
        src = (gate_pre, up_pre, hidden)[which]
        dst = (gpre, upre, hid)[which]
        return pltpu.make_async_copy(
            src.at[:, columns(b)], dst.at[b], load_sem.at[which, b]
        )

    token_copy = pltpu.make_async_copy(tokens, tok, weight_sem.at[0])
    weight_copies = (
        pltpu.make_async_copy(gate_weight, gw, weight_sem.at[1]),
        pltpu.make_async_copy(up_weight, uw, weight_sem.at[2]),
    )
    for which in range(3):
        load(which, 0).start()
    token_copy.start()

    barrier = pltpu.get_barrier_semaphore()

    @pl.when(has_left)
    def _():
        pl.semaphore_signal(barrier, inc=1, device_id={"rep": z - 1}, device_id_type=MESH)

    @pl.when(has_right)
    def _():
        pl.semaphore_signal(barrier, inc=1, device_id={"rep": z + 1}, device_id_type=MESH)

    for d in range(1, tp_count):
        peer = lax.rem(me + d, tp_count)
        pl.semaphore_signal(barrier, inc=1, device_id={"tp": peer}, device_id_type=MESH)

    def start_load(b, carry):
        for which in range(3):
            load(which, b).start()
        return carry

    lax.fori_loop(1, blocks, start_load, 0)
    for copy in weight_copies:
        copy.start()

    zero_rows = jnp.zeros((PAD, CW), F32)
    gpad[0:PAD, :] = zero_rows
    upad[0:PAD, :] = zero_rows
    gdel[length : length + PAD, :] = zero_rows
    udel[length : length + PAD, :] = zero_rows

    tile = TILE if length % TILE == 0 else length
    piece_rows = length // 3 if length % (3 * tile) == 0 else length

    def folded(x):
        return jnp.sum(x.reshape(x.shape[0] // 8, 8, CW), axis=0)

    def elementwise(b, first_row, rows):
        cols = columns(b)
        gt = [gate_taps[k : k + 1, cols] for k in range(taps)]
        ut = [up_taps[k : k + 1, cols] for k in range(taps)]
        gb = gate_bias[cols].reshape(1, CW)
        ub = up_bias[cols].reshape(1, CW)

        def mix_back(r):
            gk = gdel[r + taps - 1 : r + taps - 1 + tile, :] * gt[0]
            uk = udel[r + taps - 1 : r + taps - 1 + tile, :] * ut[0]
            for k in range(1, taps):
                first = r + taps - 1 - k
                gk = gk + gdel[first : first + tile, :] * gt[k]
                uk = uk + udel[first : first + tile, :] * ut[k]
            gback[r : r + tile, :] = gk.astype(BF16)
            uback[r : r + tile, :] = uk.astype(BF16)

        sums = None
        for r in range(first_row, first_row + rows, tile):
            g_now = gpre[b, r : r + tile, :].astype(F32)
            u_now = upre[b, r : r + tile, :].astype(F32)
            gpad[PAD + r : PAD + r + tile, :] = g_now
            upad[PAD + r : PAD + r + tile, :] = u_now
            start = PAD + r - (taps - 1)
            gs = [gpad[start + k : start + k + tile, :] for k in range(taps - 1)] + [g_now]
            us = [upad[start + k : start + k + tile, :] for k in range(taps - 1)] + [u_now]
            gm = gs[0] * gt[0]
            um = us[0] * ut[0]
            for k in range(1, taps):
                gm = gm + gs[k] * gt[k]
                um = um + us[k] * ut[k]
            gm = gm + gb
            um = um + ub
            s = jax.nn.sigmoid(gm)
            hs = hid[b, r : r + tile, :].astype(F32) * s
            gd = hs * um * (1.0 + gm * (1.0 - s))
            ud = hs * gm
            gdel[r : r + tile, :] = gd
            udel[r : r + tile, :] = ud
            parts = (
                [folded(gd * g) for g in gs]
                + [folded(ud * u) for u in us]
                + [folded(gd), folded(ud)]
            )
            sums = parts if sums is None else [a + p for a, p in zip(sums, parts)]
            if r > 0:
                mix_back(r - tile)
        last = first_row + rows == length
        if last:
            mix_back(length - tile)
        for k, part in enumerate(sums):
            if first_row > 0:
                part = part + parts_ref[k]
            if last:
                small[k : k + 1, cols] = jnp.sum(part, axis=0, keepdims=True)
            else:
                parts_ref[k] = part

    def own_right(c):
        return pltpu.make_async_remote_copy(
            src_ref=own.at[c],
            dst_ref=from_left.at[c],
            send_sem=send_r.at[c],
            recv_sem=recv_r.at[c],
            device_id={"rep": z + 1},
            device_id_type=MESH,
        )

    def own_left(c):
        return pltpu.make_async_remote_copy(
            src_ref=own.at[c],
            dst_ref=from_right.at[c],
            send_sem=send_l.at[c],
            recv_sem=recv_l.at[c],
            device_id={"rep": z - 1},
            device_id_type=MESH,
        )

    def right_copy(c):
        return pltpu.make_async_remote_copy(
            src_ref=from_left.at[c],
            dst_ref=from_left.at[c],
            send_sem=send_r.at[c],
            recv_sem=recv_r.at[c],
            device_id={"rep": z + 1},
            device_id_type=MESH,
        )

    def left_copy(c):
        return pltpu.make_async_remote_copy(
            src_ref=to_left.at[c],
            dst_ref=from_right.at[c],
            send_sem=send_l.at[c],
            recv_sem=recv_l.at[c],
            device_id={"rep": z - 1},
            device_id_type=MESH,
        )

    def weight_grad(b, first, last):
        block = jnp.concatenate([gback[...], uback[...]], axis=1)
        for q in range(first, last):
            own[b * NQ + q] = jnp.dot(
                tok_t[q * rows_q : (q + 1) * rows_q, :], block, preferred_element_type=F32
            ).astype(BF16)

    def input_grad(b, fresh):
        cols = columns(b)
        weights = jnp.concatenate([gw[:, cols], uw[:, cols]], axis=1)
        dot_rows = 256 if length % 256 == 0 else length
        for r in range(0, length, dot_rows):
            value = lax.dot_general(
                jnp.concatenate([gback[r : r + dot_rows, :], uback[r : r + dot_rows, :]], axis=1),
                weights,
                (((1,), (1,)), ((), ())),
                preferred_element_type=F32,
            )
            if fresh:
                acc[r : r + dot_rows, :] = value
            else:
                acc[r : r + dot_rows, :] += value

    small_right = pltpu.make_async_remote_copy(
        src_ref=small_to_right,
        dst_ref=small_from_left,
        send_sem=small_sem.at[0],
        recv_sem=small_sem.at[1],
        device_id={"rep": z + 1},
        device_id_type=MESH,
    )
    small_left = pltpu.make_async_remote_copy(
        src_ref=small_to_left,
        dst_ref=small_from_right,
        send_sem=small_sem.at[2],
        recv_sem=small_sem.at[3],
        device_id={"rep": z - 1},
        device_id_type=MESH,
    )

    def scatter_copy(d):
        peer = lax.rem(me + d, tp_count)
        return pltpu.make_async_remote_copy(
            src_ref=term.at[peer],
            dst_ref=term_in.at[d - 1],
            send_sem=scatter_send.at[d - 1],
            recv_sem=scatter_recv.at[d - 1],
            device_id={"tp": peer},
            device_id_type=MESH,
        )

    def gather_copy(d, slot):
        return pltpu.make_async_remote_copy(
            src_ref=final.at[slot],
            dst_ref=final.at[slot],
            send_sem=gather_send.at[d - 1],
            recv_sem=gather_recv.at[d - 1],
            device_id={"tp": lax.rem(me + d, tp_count)},
            device_id_type=MESH,
        )

    term_rows = length // tp_count

    for which in range(3):
        load(which, 0).wait()
    elementwise(0, 0, length)
    token_copy.wait()
    per_turn = max(CW // rows_q, 1)
    early = min(per_turn, NQ)

    def turn(first, last):
        for i in range(first * rows_q, last * rows_q, CW):
            tok_t[i : i + CW, :] = tok[:, i : i + CW].T

    turn(0, early)
    pl.semaphore_wait(
        barrier,
        jnp.where(has_left, 1, 0) + jnp.where(has_right, 1, 0) + (tp_count - 1),
    )
    weight_grad(0, 0, early)
    if early < NQ:
        turn(early, NQ)
        weight_grad(0, early, NQ)
    for copy in weight_copies:
        copy.wait()
    input_grad(0, True)

    @pl.when(jnp.logical_not(has_left))
    def _():
        small_from_left[...] = jnp.zeros_like(small_from_left)

    @pl.when(jnp.logical_not(has_right))
    def _():
        small_from_right[...] = jnp.zeros_like(small_from_right)

    def move(tick):
        @pl.when(jnp.logical_not(has_left) & (tick < chunks))
        def _():
            own_right(tick).start()

        @pl.when(jnp.logical_not(has_right) & (tick < chunks))
        def _():
            own_left(tick).start()

        c_right = tick - LAG * z
        c_left = tick - LAG * (rep_count - 1 - z)
        c_out = tick - LAG * (rep_count - 1)

        @pl.when(has_left & (c_right >= 0) & (c_right < chunks))
        def _():
            c = c_right
            right_copy(c).wait_recv()

            @pl.when(has_right)
            def _():
                from_left[c] = (from_left[c].astype(F32) + own[c].astype(F32)).astype(BF16)
                right_copy(c).start()

        @pl.when(has_right & (c_left >= 0) & (c_left < chunks))
        def _():
            c = c_left
            left_copy(c).wait_recv()

            @pl.when(has_left)
            def _():
                to_left[c] = (from_right[c].astype(F32) + own[c].astype(F32)).astype(BF16)
                left_copy(c).start()

        @pl.when((c_out >= 0) & (c_out < chunks))
        def _():
            c = c_out

            @pl.when(both)
            def _():
                own[c] = (from_left[c].astype(F32) + from_right[c].astype(F32)).astype(BF16)

            @pl.when(jnp.logical_not(has_left))
            def _():
                own_right(c).wait_send()
                own[c] = (own[c].astype(F32) + from_right[c].astype(F32)).astype(BF16)

            @pl.when(jnp.logical_not(has_right))
            def _():
                own_left(c).wait_send()
                own[c] = (from_left[c].astype(F32) + own[c].astype(F32)).astype(BF16)

    def step(h, carry):
        b = h + 1
        for p in range(TICKS):
            move(h * TICKS + p)

            if p * piece_rows < length:

                @pl.when(b < blocks)
                def _():
                    if p == 0:
                        for which in range(3):
                            load(which, b).wait()
                    elementwise(b, p * piece_rows, piece_rows)

            elif p == TICKS - 1:

                @pl.when(b < blocks)
                def _():
                    weight_grad(b, 0, NQ)
                    input_grad(b, False)

        @pl.when(h == done)
        def _():
            for k in range(tp_count):
                term[k] = acc[k * term_rows : (k + 1) * term_rows, :].astype(BF16)
            for d in range(1, tp_count):
                scatter_copy(d).start()

        @pl.when(h == done + 4)
        def _():
            total = term[me].astype(F32)
            for d in range(1, tp_count):
                scatter_copy(d).wait()
                total = total + term_in[d - 1].astype(F32)
            final[me] = total.astype(BF16)
            for d in range(1, tp_count):
                gather_copy(d, me).start()

        @pl.when(h == done + z)
        def _():
            @pl.when(has_left)
            def _():
                small_right.wait_recv()

            @pl.when(has_right)
            def _():
                small_to_right[...] = small_from_left[...] + small[...]
                small_right.start()

        @pl.when(h == done + rep_count - 1 - z)
        def _():
            @pl.when(has_right)
            def _():
                small_left.wait_recv()

            @pl.when(has_left)
            def _():
                small_to_left[...] = small_from_right[...] + small[...]
                small_left.start()

        return carry

    lax.fori_loop(0, steps, step, 0)

    small_out[...] = small_from_left[...] + small[...] + small_from_right[...]
    for d in range(1, tp_count):
        gather_copy(d, lax.rem(me + tp_count - d, tp_count)).wait_recv()
    for d in range(1, tp_count):
        gather_copy(d, me).wait_send()

    @pl.when(has_right)
    def _():
        small_right.wait_send()

    @pl.when(has_left)
    def _():
        small_left.wait_send()

    @pl.when(both)
    def _():
        def drain(c, carry):
            right_copy(c).wait_send()
            left_copy(c).wait_send()
            return carry

        lax.fori_loop(0, chunks, drain, 0)


def spread(
    chunks_ref, final, small, grad_out, gate_out, up_out, gate_taps_out, up_taps_out,
    gate_bias_out, up_bias_out, gate_rows, up_rows, gate_small, up_small, gate_line,
    up_line, row_sem, grad_sem, small_sem,
):
    blocks = gate_out.shape[1] // CW
    rows_q = gate_out.shape[0] // NQ
    taps = gate_taps_out.shape[0]
    slots, term_rows = final.shape[0], final.shape[1]

    def rows_copy(which, q):
        return pltpu.make_async_copy(
            (gate_rows, up_rows)[which].at[q % 2],
            (gate_out, up_out)[which].at[q * rows_q : (q + 1) * rows_q, :],
            row_sem.at[which, q],
        )

    for q in range(NQ):
        if q >= 2:
            rows_copy(0, q - 2).wait()
            rows_copy(1, q - 2).wait()
        for b in range(blocks):
            chunk = chunks_ref[b * NQ + q]
            gate_rows[q % 2, :, b * CW : (b + 1) * CW] = chunk[:, 0:CW].astype(F32)
            up_rows[q % 2, :, b * CW : (b + 1) * CW] = chunk[:, CW : 2 * CW].astype(F32)
        rows_copy(0, q).start()
        rows_copy(1, q).start()

    gate_small[...] = small[0:taps, :]
    up_small[...] = small[taps : 2 * taps, :]
    gate_line[...] = small[2 * taps, :]
    up_line[...] = small[2 * taps + 1, :]
    copies = [
        pltpu.make_async_copy(
            final.at[k], grad_out.at[k * term_rows : (k + 1) * term_rows, :], grad_sem.at[k]
        )
        for k in range(slots)
    ] + [
        pltpu.make_async_copy(gate_small, gate_taps_out, small_sem.at[0]),
        pltpu.make_async_copy(up_small, up_taps_out, small_sem.at[1]),
        pltpu.make_async_copy(gate_line, gate_bias_out, small_sem.at[2]),
        pltpu.make_async_copy(up_line, up_bias_out, small_sem.at[3]),
    ]
    for copy in copies:
        copy.start()
    for copy in copies:
        copy.wait()
    for q in range(max(NQ - 2, 0), NQ):
        rows_copy(0, q).wait()
        rows_copy(1, q).wait()


def per_device(
    rep_count,
    tp_count,
    tokens,
    gate_pre,
    up_pre,
    hidden_grad,
    gate_weight,
    up_weight,
    gate_taps,
    up_taps,
    gate_bias,
    up_bias,
):
    length, hidden_cols = gate_pre.shape
    width = tokens.shape[1]
    taps = gate_taps.shape[0]
    blocks = hidden_cols // CW
    chunks = blocks * NQ
    rows_q = width // NQ
    term_rows = length // tp_count
    small_rows = 2 * taps + 2
    anywhere = pl.BlockSpec(memory_space=pl.ANY)
    vmem = pl.BlockSpec(memory_space=pltpu.VMEM)
    line = pltpu.VMEM((chunks, rows_q, 2 * CW), BF16)
    small = pltpu.VMEM((small_rows, hidden_cols), F32)
    dma = pltpu.SemaphoreType.DMA
    summed, final, small_sum = pl.pallas_call(
        functools.partial(fused, rep_count, tp_count),
        out_shape=(
            pltpu.VMEM((chunks, rows_q, 2 * CW), BF16),
            pltpu.VMEM((tp_count, term_rows, width), BF16),
            pltpu.VMEM((small_rows, hidden_cols), F32),
        ),
        in_specs=[anywhere] * 6 + [vmem] * 4,
        out_specs=(vmem, vmem, vmem),
        scratch_shapes=[
            pltpu.VMEM((length, width), BF16),
            pltpu.VMEM((width, length), BF16),
            pltpu.VMEM((blocks, length, CW), BF16),
            pltpu.VMEM((blocks, length, CW), BF16),
            pltpu.VMEM((blocks, length, CW), BF16),
            pltpu.VMEM((width, hidden_cols), BF16),
            pltpu.VMEM((width, hidden_cols), BF16),
            pltpu.VMEM((PAD + length, CW), F32),
            pltpu.VMEM((PAD + length, CW), F32),
            pltpu.VMEM((length + PAD, CW), F32),
            pltpu.VMEM((length + PAD, CW), F32),
            pltpu.VMEM((length, CW), BF16),
            pltpu.VMEM((length, CW), BF16),
            pltpu.VMEM((small_rows, 8, CW), F32),
            pltpu.VMEM((length, width), F32),
            line,
            line,
            line,
            pltpu.VMEM((tp_count, term_rows, width), BF16),
            pltpu.VMEM((tp_count - 1, term_rows, width), BF16),
            small,
            small,
            small,
            small,
            small,
            dma((3, blocks)),
            dma((3,)),
            dma((chunks,)),
            dma((chunks,)),
            dma((chunks,)),
            dma((chunks,)),
            dma((tp_count - 1,)),
            dma((tp_count - 1,)),
            dma((tp_count - 1,)),
            dma((tp_count - 1,)),
            dma((4,)),
        ],
        compiler_params=pltpu.CompilerParams(
            collective_id=0, has_side_effects=True, vmem_limit_bytes=48 * 2**20
        ),
    )(
        tokens,
        gate_pre,
        up_pre,
        hidden_grad,
        gate_weight,
        up_weight,
        gate_taps,
        up_taps,
        gate_bias,
        up_bias,
    )
    held = [pltpu.with_memory_space_constraint(x, pltpu.VMEM) for x in (summed, final, small_sum)]
    return pl.pallas_call(
        spread,
        out_shape=(
            jax.ShapeDtypeStruct((length, width), BF16),
            jax.ShapeDtypeStruct((width, hidden_cols), F32),
            jax.ShapeDtypeStruct((width, hidden_cols), F32),
            jax.ShapeDtypeStruct((taps, hidden_cols), F32),
            jax.ShapeDtypeStruct((taps, hidden_cols), F32),
            jax.ShapeDtypeStruct((hidden_cols,), F32),
            jax.ShapeDtypeStruct((hidden_cols,), F32),
        ),
        in_specs=[vmem] * 3,
        out_specs=[anywhere] * 7,
        scratch_shapes=[
            pltpu.VMEM((2, rows_q, hidden_cols), F32),
            pltpu.VMEM((2, rows_q, hidden_cols), F32),
            pltpu.VMEM((taps, hidden_cols), F32),
            pltpu.VMEM((taps, hidden_cols), F32),
            pltpu.VMEM((hidden_cols,), F32),
            pltpu.VMEM((hidden_cols,), F32),
            dma((2, NQ)),
            dma((tp_count,)),
            dma((4,)),
        ],
        compiler_params=pltpu.CompilerParams(vmem_limit_bytes=8 * 2**20),
    )(*held)


def solution(mesh):
    return jax.shard_map(
        functools.partial(per_device, mesh.shape["rep"], mesh.shape["tp"]),
        mesh=mesh,
        in_specs=(
            P("rep", "fs"),
            P("rep", "tp"),
            P("rep", "tp"),
            P("rep", "tp"),
            P("fs", "tp"),
            P("fs", "tp"),
            P(None, "tp"),
            P(None, "tp"),
            P("tp"),
            P("tp"),
        ),
        out_specs=(
            P("rep", "fs"),
            P("fs", "tp"),
            P("fs", "tp"),
            P(None, "tp"),
            P(None, "tp"),
            P("tp"),
            P("tp"),
        ),
        check_vma=False,
    )
```

time: 181 us -> 167 us (0.923)
  other arithmetic: 9.19 us -> 0 us
  Pallas kernels: 169 us -> 166 us
  local copies, waits for them, and re-layouts: 2.41 us -> 0 us
    convert_element_type x2 -> x0, other arithmetic: 9.19 us -> none  [the longest x1 5.62 us: per_device(): gate_sum.astype(F32)]
    pallas_call x1, Pallas kernels: 169 us -> 160 us  [per_device(): pl.pallas_call(functools.partial(fused, rep_count, tp_count), out_shape=(...]
    pallas_call x0 -> x1, Pallas kernels: none -> 6.18 us  [per_device(): pl.pallas_call(spread, out_shape=(jax.ShapeDtypeStruct((length, width), B...]
where the time goes in v1:
time: 167 us
  Pallas kernels  166 us (99%)
    pallas_call x1, Pallas kernels, per_device(): pl.pallas_call(functools.partial(fused, rep_count, tp_count), out_shape=(...  160 us
    pallas_call x1, Pallas kernels, per_device(): pl.pallas_call(spread, out_shape=(jax.ShapeDtypeStruct((length, width), B...  6.18 us

profile of v1, /device:TPU:0, one launch (start us, length us, event | category | flops | bytes accessed | tf_op | source)
XLA Modules:
  0.0 166.6 jit_solution(7856296401404994633)
XLA Ops:
  0.6 159.8 %shard_map.153 = (bf16[96,128,256]{2,1,0:T(8,128)(2,1)S(1)}, bf16[4,192,1024]{2,1,0:T(8,128)(2,1)S(1)}, f32[8,1536]{1,0:T(8,128)S(1)}) custom-call(bf16[768,1024]{1,0:T(8,128)(2,1)} %tokens.1, bf16[768,1536]{1,0:T(8,128)(2,1)} %gate_pre.1, bf16[768,1536]{1,0:T(8,128)(2,1)} %up_pre.1, bf16[768,1536]{1,0:T(8,128)(2,1)} %hidden.1, ...), custom_call_target="tpu_custom_call" | custom-call | tf_op jit(solution)/shard_map/pallas_call | solution.py:559
  160.4 6.2 %shard_map.154 = (bf16[768,1024]{1,0:T(8,128)(2,1)}, f32[1024,1536]{1,0:T(8,128)}, f32[1024,1536]{1,0:T(8,128)}, f32[3,1536]{1,0:T(4,128)}, f32[3,1536]{1,0:T(4,128)}, /*index=5*/f32[1536]{0:T(1024)}, f32[1536]{0:T(1024)}) custom-call(bf16[96,128,256]{2,1,0:T(8,128)(2,1)S(1)} %get-tuple-element.10.chunks_ref, ...), custom_call_target="tpu_custom_call" | custom-call | tf_op jit(solution)/shard_map/pallas_call | solution.py:622

commit v2 on v1

--- a/solution.py
+++ b/solution.py
@@ -13,6 +13,8 @@
 PAD = 8
 TICKS = 4
 LAG = 4
+WINDOW = 2
+SLOTS = 3
 TILE = 32
 F32 = jnp.float32
 BF16 = jnp.bfloat16
@@ -34,10 +36,10 @@
     hidden,
     gate_weight,
     up_weight,
-    gate_taps,
-    up_taps,
-    gate_bias,
-    up_bias,
+    gate_taps_hbm,
+    up_taps_hbm,
+    gate_bias_hbm,
+    up_bias_hbm,
     own,
     final,
     small_out,
@@ -61,6 +63,10 @@
     to_left,
     term,
     term_in,
+    gate_taps,
+    up_taps,
+    gate_bias,
+    up_bias,
     small,
     small_from_left,
     small_from_right,
@@ -87,6 +93,7 @@
     rows_q = width // NQ
     taps = gate_taps.shape[0]
     done, steps = schedule(blocks, rep_count)
+    ring = recv_r.shape[0]
     has_left = z > 0
     has_right = z < rep_count - 1
     both = has_left & has_right
@@ -98,7 +105,7 @@
         src = (gate_pre, up_pre, hidden)[which]
         dst = (gpre, upre, hid)[which]
         return pltpu.make_async_copy(
-            src.at[:, columns(b)], dst.at[b], load_sem.at[which, b]
+            src.at[:, columns(b)], dst.at[b], load_sem.at[which, lax.rem(b, SLOTS)]
         )
 
     token_copy = pltpu.make_async_copy(tokens, tok, weight_sem.at[0])
@@ -106,8 +113,21 @@
         pltpu.make_async_copy(gate_weight, gw, weight_sem.at[1]),
         pltpu.make_async_copy(up_weight, uw, weight_sem.at[2]),
     )
+    small_copies = [
+        pltpu.make_async_copy(src, dst, weight_sem.at[3 + i])
+        for i, (src, dst) in enumerate(
+            (
+                (gate_taps_hbm, gate_taps),
+                (up_taps_hbm, up_taps),
+                (gate_bias_hbm, gate_bias),
+                (up_bias_hbm, up_bias),
+            )
+        )
+    ]
     for which in range(3):
         load(which, 0).start()
+    for copy in small_copies:
+        copy.start()
     token_copy.start()
 
     barrier = pltpu.get_barrier_semaphore()
@@ -129,7 +149,8 @@
             load(which, b).start()
         return carry
 
-    lax.fori_loop(1, blocks, start_load, 0)
+    for b in range(1, min(SLOTS, blocks)):
+        start_load(b, 0)
     for copy in weight_copies:
         copy.start()
 
@@ -207,8 +228,8 @@
         return pltpu.make_async_remote_copy(
             src_ref=own.at[c],
             dst_ref=from_left.at[c],
-            send_sem=send_r.at[c],
-            recv_sem=recv_r.at[c],
+            send_sem=send_r.at[lax.rem(c, WINDOW)],
+            recv_sem=recv_r.at[lax.rem(c, ring)],
             device_id={"rep": z + 1},
             device_id_type=MESH,
         )
@@ -217,8 +238,8 @@
         return pltpu.make_async_remote_copy(
             src_ref=own.at[c],
             dst_ref=from_right.at[c],
-            send_sem=send_l.at[c],
-            recv_sem=recv_l.at[c],
+            send_sem=send_l.at[lax.rem(c, WINDOW)],
+            recv_sem=recv_l.at[lax.rem(c, ring)],
             device_id={"rep": z - 1},
             device_id_type=MESH,
         )
@@ -227,8 +248,8 @@
         return pltpu.make_async_remote_copy(
             src_ref=from_left.at[c],
             dst_ref=from_left.at[c],
-            send_sem=send_r.at[c],
-            recv_sem=recv_r.at[c],
+            send_sem=send_r.at[lax.rem(c, WINDOW)],
+            recv_sem=recv_r.at[lax.rem(c, ring)],
             device_id={"rep": z + 1},
             device_id_type=MESH,
         )
@@ -237,8 +258,8 @@
         return pltpu.make_async_remote_copy(
             src_ref=to_left.at[c],
             dst_ref=from_right.at[c],
-            send_sem=send_l.at[c],
-            recv_sem=recv_l.at[c],
+            send_sem=send_l.at[lax.rem(c, WINDOW)],
+            recv_sem=recv_l.at[lax.rem(c, ring)],
             device_id={"rep": z - 1},
             device_id_type=MESH,
         )
@@ -308,6 +329,8 @@
 
     for which in range(3):
         load(which, 0).wait()
+    for copy in small_copies:
+        copy.wait()
     elementwise(0, 0, length)
     token_copy.wait()
     per_turn = max(CW // rows_q, 1)
@@ -339,34 +362,48 @@
         small_from_right[...] = jnp.zeros_like(small_from_right)
 
     def move(tick):
-        @pl.when(jnp.logical_not(has_left) & (tick < chunks))
-        def _():
-            own_right(tick).start()
-
-        @pl.when(jnp.logical_not(has_right) & (tick < chunks))
-        def _():
-            own_left(tick).start()
-
         c_right = tick - LAG * z
         c_left = tick - LAG * (rep_count - 1 - z)
         c_out = tick - LAG * (rep_count - 1)
 
-        @pl.when(has_left & (c_right >= 0) & (c_right < chunks))
+        @pl.when(has_right & (c_right >= WINDOW) & (c_right < chunks + WINDOW))
+        def _():
+            right_copy(c_right - WINDOW).wait_send()
+
+        @pl.when((c_right >= 0) & (c_right < chunks))
         def _():
             c = c_right
-            right_copy(c).wait_recv()
-
-            @pl.when(has_right)
+
+            @pl.when(jnp.logical_not(has_left))
+            def _():
+                own_right(c).start()
+
+            @pl.when(has_left)
+            def _():
+                right_copy(c).wait_recv()
+
+            @pl.when(both)
             def _():
                 from_left[c] = (from_left[c].astype(F32) + own[c].astype(F32)).astype(BF16)
                 right_copy(c).start()
 
-        @pl.when(has_right & (c_left >= 0) & (c_left < chunks))
+        @pl.when(has_left & (c_left >= WINDOW) & (c_left < chunks + WINDOW))
+        def _():
+            left_copy(c_left - WINDOW).wait_send()
+
+        @pl.when((c_left >= 0) & (c_left < chunks))
         def _():
             c = c_left
-            left_copy(c).wait_recv()
-
-            @pl.when(has_left)
+
+            @pl.when(jnp.logical_not(has_right))
+            def _():
+                own_left(c).start()
+
+            @pl.when(has_right)
+            def _():
+                left_copy(c).wait_recv()
+
+            @pl.when(both)
             def _():
                 to_left[c] = (from_right[c].astype(F32) + own[c].astype(F32)).astype(BF16)
                 left_copy(c).start()
@@ -381,12 +418,10 @@
 
             @pl.when(jnp.logical_not(has_left))
             def _():
-                own_right(c).wait_send()
                 own[c] = (own[c].astype(F32) + from_right[c].astype(F32)).astype(BF16)
 
             @pl.when(jnp.logical_not(has_right))
             def _():
-                own_left(c).wait_send()
                 own[c] = (from_left[c].astype(F32) + own[c].astype(F32)).astype(BF16)
 
     def step(h, carry):
@@ -401,6 +436,11 @@
                     if p == 0:
                         for which in range(3):
                             load(which, b).wait()
+
+                        @pl.when(b + SLOTS - 1 < blocks)
+                        def _():
+                            start_load(b + SLOTS - 1, 0)
+
                     elementwise(b, p * piece_rows, piece_rows)
 
             elif p == TICKS - 1:
@@ -435,7 +475,7 @@
 
             @pl.when(has_right)
             def _():
-                small_to_right[...] = small_from_left[...] + small[...]
+                small_to_right[...] = (small_from_left[...].astype(F32) + small[...]).astype(BF16)
                 small_right.start()
 
         @pl.when(h == done + rep_count - 1 - z)
@@ -446,14 +486,14 @@
 
             @pl.when(has_left)
             def _():
-                small_to_left[...] = small_from_right[...] + small[...]
+                small_to_left[...] = (small_from_right[...].astype(F32) + small[...]).astype(BF16)
                 small_left.start()
 
         return carry
 
     lax.fori_loop(0, steps, step, 0)
 
-    small_out[...] = small_from_left[...] + small[...] + small_from_right[...]
+    small_out[...] = small_from_left[...].astype(F32) + small[...] + small_from_right[...].astype(F32)
     for d in range(1, tp_count):
         gather_copy(d, lax.rem(me + tp_count - d, tp_count)).wait_recv()
     for d in range(1, tp_count):
@@ -466,15 +506,6 @@
     @pl.when(has_left)
     def _():
         small_left.wait_send()
-
-    @pl.when(both)
-    def _():
-        def drain(c, carry):
-            right_copy(c).wait_send()
-            left_copy(c).wait_send()
-            return carry
-
-        lax.fori_loop(0, chunks, drain, 0)
 
 
 def spread(
@@ -489,21 +520,10 @@
 
     def rows_copy(which, q):
         return pltpu.make_async_copy(
-            (gate_rows, up_rows)[which].at[q % 2],
+            (gate_rows, up_rows)[which].at[q],
             (gate_out, up_out)[which].at[q * rows_q : (q + 1) * rows_q, :],
             row_sem.at[which, q],
         )
-
-    for q in range(NQ):
-        if q >= 2:
-            rows_copy(0, q - 2).wait()
-            rows_copy(1, q - 2).wait()
-        for b in range(blocks):
-            chunk = chunks_ref[b * NQ + q]
-            gate_rows[q % 2, :, b * CW : (b + 1) * CW] = chunk[:, 0:CW].astype(F32)
-            up_rows[q % 2, :, b * CW : (b + 1) * CW] = chunk[:, CW : 2 * CW].astype(F32)
-        rows_copy(0, q).start()
-        rows_copy(1, q).start()
 
     gate_small[...] = small[0:taps, :]
     up_small[...] = small[taps : 2 * taps, :]
@@ -522,9 +542,16 @@
     ]
     for copy in copies:
         copy.start()
+    for q in range(NQ):
+        for b in range(blocks):
+            chunk = chunks_ref[b * NQ + q]
+            gate_rows[q, :, b * CW : (b + 1) * CW] = chunk[:, 0:CW].astype(F32)
+            up_rows[q, :, b * CW : (b + 1) * CW] = chunk[:, CW : 2 * CW].astype(F32)
+        rows_copy(0, q).start()
+        rows_copy(1, q).start()
     for copy in copies:
         copy.wait()
-    for q in range(max(NQ - 2, 0), NQ):
+    for q in range(NQ):
         rows_copy(0, q).wait()
         rows_copy(1, q).wait()
 
@@ -550,11 +577,13 @@
     chunks = blocks * NQ
     rows_q = width // NQ
     term_rows = length // tp_count
+    ring = min(chunks, LAG * (rep_count - 1) + TICKS)
     small_rows = 2 * taps + 2
     anywhere = pl.BlockSpec(memory_space=pl.ANY)
     vmem = pl.BlockSpec(memory_space=pltpu.VMEM)
     line = pltpu.VMEM((chunks, rows_q, 2 * CW), BF16)
     small = pltpu.VMEM((small_rows, hidden_cols), F32)
+    small_line = pltpu.VMEM((small_rows, hidden_cols), BF16)
     dma = pltpu.SemaphoreType.DMA
     summed, final, small_sum = pl.pallas_call(
         functools.partial(fused, rep_count, tp_count),
@@ -563,7 +592,7 @@
             pltpu.VMEM((tp_count, term_rows, width), BF16),
             pltpu.VMEM((small_rows, hidden_cols), F32),
         ),
-        in_specs=[anywhere] * 6 + [vmem] * 4,
+        in_specs=[anywhere] * 10,
         out_specs=(vmem, vmem, vmem),
         scratch_shapes=[
             pltpu.VMEM((length, width), BF16),
@@ -586,17 +615,21 @@
             line,
             pltpu.VMEM((tp_count, term_rows, width), BF16),
             pltpu.VMEM((tp_count - 1, term_rows, width), BF16),
+            pltpu.VMEM((taps, hidden_cols), F32),
+            pltpu.VMEM((taps, hidden_cols), F32),
+            pltpu.VMEM((hidden_cols,), F32),
+            pltpu.VMEM((hidden_cols,), F32),
             small,
-            small,
-            small,
-            small,
-            small,
-            dma((3, blocks)),
-            dma((3,)),
-            dma((chunks,)),
-            dma((chunks,)),
-            dma((chunks,)),
-            dma((chunks,)),
+            small_line,
+            small_line,
+            small_line,
+            small_line,
+            dma((3, SLOTS)),
+            dma((7,)),
+            dma((WINDOW,)),
+            dma((ring,)),
+            dma((WINDOW,)),
+            dma((ring,)),
             dma((tp_count - 1,)),
             dma((tp_count - 1,)),
             dma((tp_count - 1,)),
@@ -633,8 +666,8 @@
         in_specs=[vmem] * 3,
         out_specs=[anywhere] * 7,
         scratch_shapes=[
-            pltpu.VMEM((2, rows_q, hidden_cols), F32),
-            pltpu.VMEM((2, rows_q, hidden_cols), F32),
+            pltpu.VMEM((NQ, rows_q, hidden_cols), F32),
+            pltpu.VMEM((NQ, rows_q, hidden_cols), F32),
             pltpu.VMEM((taps, hidden_cols), F32),
             pltpu.VMEM((taps, hidden_cols), F32),
             pltpu.VMEM((hidden_cols,), F32),
@@ -643,7 +676,7 @@
             dma((tp_count,)),
             dma((4,)),
         ],
-        compiler_params=pltpu.CompilerParams(vmem_limit_bytes=8 * 2**20),
+        compiler_params=pltpu.CompilerParams(vmem_limit_bytes=16 * 2**20),
     )(*held)
 
 

time: 167 us -> 159 us (0.952)
  Pallas kernels: 166 us -> 159 us
    pallas_call x1, Pallas kernels: 160 us -> 153 us  [per_device(): pl.pallas_call(functools.partial(fused, rep_count, tp_count), out_shape=(...]
where the time goes in v2:
time: 159 us
  Pallas kernels  159 us (100%)
    pallas_call x1, Pallas kernels, per_device(): pl.pallas_call(functools.partial(fused, rep_count, tp_count), out_shape=(...  153 us
    pallas_call x1, Pallas kernels, per_device(): pl.pallas_call(spread, out_shape=(jax.ShapeDtypeStruct((length, width), B...  5.39 us

profile of v2, /device:TPU:0, one launch (start us, length us, event | category | flops | bytes accessed | tf_op | source)
XLA Modules:
  0.0 159.2 jit_solution(5011636375620904456)
XLA Ops:
  0.6 153.2 %shard_map.153 = (bf16[96,128,256]{2,1,0:T(8,128)(2,1)S(1)}, bf16[4,192,1024]{2,1,0:T(8,128)(2,1)S(1)}, f32[8,1536]{1,0:T(8,128)S(1)}) custom-call(bf16[768,1024]{1,0:T(8,128)(2,1)} %tokens.1, bf16[768,1536]{1,0:T(8,128)(2,1)} %gate_pre.1, bf16[768,1536]{1,0:T(8,128)(2,1)} %up_pre.1, bf16[768,1536]{1,0:T(8,128)(2,1)} %hidden.1, ...), custom_call_target="tpu_custom_call" | custom-call | tf_op jit(solution)/shard_map/pallas_call | solution.py:588
  153.8 5.4 %shard_map.154 = (bf16[768,1024]{1,0:T(8,128)(2,1)}, f32[1024,1536]{1,0:T(8,128)}, f32[1024,1536]{1,0:T(8,128)}, f32[3,1536]{1,0:T(4,128)}, f32[3,1536]{1,0:T(4,128)}, /*index=5*/f32[1536]{0:T(1024)}, f32[1536]{0:T(1024)}) custom-call(bf16[96,128,256]{2,1,0:T(8,128)(2,1)S(1)} %get-tuple-element.10.chunks_ref, ...), custom_call_target="tpu_custom_call" | custom-call | tf_op jit(solution)/shard_map/pallas_call | solution.py:655

commit v3 on v2

--- a/solution.py
+++ b/solution.py
@@ -11,9 +11,10 @@
 CW = 128
 NQ = 8
 PAD = 8
-TICKS = 4
-LAG = 4
-WINDOW = 2
+TICKS = NQ // 2
+PIECE = TICKS // 4
+LAG = 3
+WINDOW = 3
 SLOTS = 3
 TILE = 32
 F32 = jnp.float32
@@ -21,9 +22,9 @@
 
 
 def schedule(blocks, rep_count):
-    done = max(blocks - 1, 0)
+    done = blocks
     last_tick = blocks * NQ + LAG * (rep_count - 1)
-    steps = max(-(-last_tick // TICKS), done + rep_count, done + 5)
+    steps = max(-(-(last_tick - 1) // TICKS), done + 2 * rep_count, done + rep_count + 4)
     return done, steps
 
 
@@ -98,6 +99,20 @@
     has_right = z < rep_count - 1
     both = has_left & has_right
 
+    barrier = pltpu.get_barrier_semaphore()
+
+    @pl.when(has_left)
+    def _():
+        pl.semaphore_signal(barrier, inc=1, device_id={"rep": z - 1}, device_id_type=MESH)
+
+    @pl.when(has_right)
+    def _():
+        pl.semaphore_signal(barrier, inc=1, device_id={"rep": z + 1}, device_id_type=MESH)
+
+    for d in range(1, tp_count):
+        peer = lax.rem(me + d, tp_count)
+        pl.semaphore_signal(barrier, inc=1, device_id={"tp": peer}, device_id_type=MESH)
+
     def columns(b):
         return pl.ds(pl.multiple_of(b * CW, CW), CW)
 
@@ -108,7 +123,10 @@
             src.at[:, columns(b)], dst.at[b], load_sem.at[which, lax.rem(b, SLOTS)]
         )
 
-    token_copy = pltpu.make_async_copy(tokens, tok, weight_sem.at[0])
+    token_copies = [
+        pltpu.make_async_copy(tokens.at[:, part], tok.at[:, part], weight_sem.at[i])
+        for i, part in ((0, pl.ds(0, CW)), (7, pl.ds(CW, width - CW)))
+    ]
     weight_copies = (
         pltpu.make_async_copy(gate_weight, gw, weight_sem.at[1]),
         pltpu.make_async_copy(up_weight, uw, weight_sem.at[2]),
@@ -128,31 +146,13 @@
         load(which, 0).start()
     for copy in small_copies:
         copy.start()
-    token_copy.start()
-
-    barrier = pltpu.get_barrier_semaphore()
-
-    @pl.when(has_left)
-    def _():
-        pl.semaphore_signal(barrier, inc=1, device_id={"rep": z - 1}, device_id_type=MESH)
-
-    @pl.when(has_right)
-    def _():
-        pl.semaphore_signal(barrier, inc=1, device_id={"rep": z + 1}, device_id_type=MESH)
-
-    for d in range(1, tp_count):
-        peer = lax.rem(me + d, tp_count)
-        pl.semaphore_signal(barrier, inc=1, device_id={"tp": peer}, device_id_type=MESH)
+    for copy in token_copies:
+        copy.start()
 
     def start_load(b, carry):
         for which in range(3):
             load(which, b).start()
         return carry
-
-    for b in range(1, min(SLOTS, blocks)):
-        start_load(b, 0)
-    for copy in weight_copies:
-        copy.start()
 
     zero_rows = jnp.zeros((PAD, CW), F32)
     gpad[0:PAD, :] = zero_rows
@@ -161,7 +161,6 @@
     udel[length : length + PAD, :] = zero_rows
 
     tile = TILE if length % TILE == 0 else length
-    piece_rows = length // 3 if length % (3 * tile) == 0 else length
 
     def folded(x):
         return jnp.sum(x.reshape(x.shape[0] // 8, 8, CW), axis=0)
@@ -271,11 +270,12 @@
                 tok_t[q * rows_q : (q + 1) * rows_q, :], block, preferred_element_type=F32
             ).astype(BF16)
 
-    def input_grad(b, fresh):
+    dot_rows = 256 if length % 256 == 0 else length
+
+    def input_grad(b, fresh, begin, end):
         cols = columns(b)
         weights = jnp.concatenate([gw[:, cols], uw[:, cols]], axis=1)
-        dot_rows = 256 if length % 256 == 0 else length
-        for r in range(0, length, dot_rows):
+        for r in range(begin, end, dot_rows):
             value = lax.dot_general(
                 jnp.concatenate([gback[r : r + dot_rows, :], uback[r : r + dot_rows, :]], axis=1),
                 weights,
@@ -327,12 +327,74 @@
 
     term_rows = length // tp_count
 
+    def move(tick):
+        c_right = tick - LAG * z
+        c_left = tick - LAG * (rep_count - 1 - z)
+        c_out = tick - LAG * (rep_count - 1)
+
+        @pl.when(has_left & (c_left >= WINDOW) & (c_left < chunks + WINDOW))
+        def _():
+            left_copy(c_left - WINDOW).wait_send()
+
+        @pl.when((c_left >= 0) & (c_left < chunks))
+        def _():
+            c = c_left
+
+            @pl.when(jnp.logical_not(has_right))
+            def _():
+                own_left(c).start()
+
+            @pl.when(has_right)
+            def _():
+                left_copy(c).wait_recv()
+
+            @pl.when(both)
+            def _():
+                to_left[c] = (from_right[c].astype(F32) + own[c].astype(F32)).astype(BF16)
+                left_copy(c).start()
+
+        @pl.when(has_right & (c_right >= WINDOW) & (c_right < chunks + WINDOW))
+        def _():
+            right_copy(c_right - WINDOW).wait_send()
+
+        @pl.when((c_right >= 0) & (c_right < chunks))
+        def _():
+            c = c_right
+
+            @pl.when(jnp.logical_not(has_left))
+            def _():
+                own_right(c).start()
+
+            @pl.when(has_left)
+            def _():
+                right_copy(c).wait_recv()
+
+            @pl.when(both)
+            def _():
+                from_left[c] = (from_left[c].astype(F32) + own[c].astype(F32)).astype(BF16)
+                right_copy(c).start()
+
+        @pl.when((c_out >= 0) & (c_out < chunks))
+        def _():
+            c = c_out
+
+            @pl.when(both)
+            def _():
+                own[c] = (from_left[c].astype(F32) + from_right[c].astype(F32)).astype(BF16)
+
+            @pl.when(jnp.logical_not(has_left))
+            def _():
+                own[c] = (own[c].astype(F32) + from_right[c].astype(F32)).astype(BF16)
+
+            @pl.when(jnp.logical_not(has_right))
+            def _():
+                own[c] = (from_left[c].astype(F32) + own[c].astype(F32)).astype(BF16)
+
     for which in range(3):
         load(which, 0).wait()
     for copy in small_copies:
         copy.wait()
     elementwise(0, 0, length)
-    token_copy.wait()
     per_turn = max(CW // rows_q, 1)
     early = min(per_turn, NQ)
 
@@ -340,18 +402,22 @@
         for i in range(first * rows_q, last * rows_q, CW):
             tok_t[i : i + CW, :] = tok[:, i : i + CW].T
 
+    token_copies[0].wait()
     turn(0, early)
+    weight_grad(0, 0, early)
     pl.semaphore_wait(
         barrier,
         jnp.where(has_left, 1, 0) + jnp.where(has_right, 1, 0) + (tp_count - 1),
     )
-    weight_grad(0, 0, early)
+    move(0)
+    token_copies[1].wait()
+    for b in range(1, min(SLOTS, blocks)):
+        start_load(b, 0)
+    for copy in weight_copies:
+        copy.start()
     if early < NQ:
         turn(early, NQ)
         weight_grad(0, early, NQ)
-    for copy in weight_copies:
-        copy.wait()
-    input_grad(0, True)
 
     @pl.when(jnp.logical_not(has_left))
     def _():
@@ -361,94 +427,37 @@
     def _():
         small_from_right[...] = jnp.zeros_like(small_from_right)
 
-    def move(tick):
-        c_right = tick - LAG * z
-        c_left = tick - LAG * (rep_count - 1 - z)
-        c_out = tick - LAG * (rep_count - 1)
-
-        @pl.when(has_right & (c_right >= WINDOW) & (c_right < chunks + WINDOW))
-        def _():
-            right_copy(c_right - WINDOW).wait_send()
-
-        @pl.when((c_right >= 0) & (c_right < chunks))
-        def _():
-            c = c_right
-
-            @pl.when(jnp.logical_not(has_left))
-            def _():
-                own_right(c).start()
-
-            @pl.when(has_left)
-            def _():
-                right_copy(c).wait_recv()
-
-            @pl.when(both)
-            def _():
-                from_left[c] = (from_left[c].astype(F32) + own[c].astype(F32)).astype(BF16)
-                right_copy(c).start()
-
-        @pl.when(has_left & (c_left >= WINDOW) & (c_left < chunks + WINDOW))
-        def _():
-            left_copy(c_left - WINDOW).wait_send()
-
-        @pl.when((c_left >= 0) & (c_left < chunks))
-        def _():
-            c = c_left
-
-            @pl.when(jnp.logical_not(has_right))
-            def _():
-                own_left(c).start()
-
-            @pl.when(has_right)
-            def _():
-                left_copy(c).wait_recv()
-
-            @pl.when(both)
-            def _():
-                to_left[c] = (from_right[c].astype(F32) + own[c].astype(F32)).astype(BF16)
-                left_copy(c).start()
-
-        @pl.when((c_out >= 0) & (c_out < chunks))
-        def _():
-            c = c_out
-
-            @pl.when(both)
-            def _():
-                own[c] = (from_left[c].astype(F32) + from_right[c].astype(F32)).astype(BF16)
-
-            @pl.when(jnp.logical_not(has_left))
-            def _():
-                own[c] = (own[c].astype(F32) + from_right[c].astype(F32)).astype(BF16)
-
-            @pl.when(jnp.logical_not(has_right))
-            def _():
-                own[c] = (from_left[c].astype(F32) + own[c].astype(F32)).astype(BF16)
-
     def step(h, carry):
-        b = h + 1
+        b = h
         for p in range(TICKS):
-            move(h * TICKS + p)
-
-            if p * piece_rows < length:
-
-                @pl.when(b < blocks)
+            move(h * TICKS + p + 1)
+
+            if p == TICKS // 2:
+
+                @pl.when(h == 0)
                 def _():
-                    if p == 0:
-                        for which in range(3):
-                            load(which, b).wait()
-
-                        @pl.when(b + SLOTS - 1 < blocks)
-                        def _():
-                            start_load(b + SLOTS - 1, 0)
-
-                    elementwise(b, p * piece_rows, piece_rows)
-
-            elif p == TICKS - 1:
-
-                @pl.when(b < blocks)
-                def _():
+                    for copy in weight_copies:
+                        copy.wait()
+                    input_grad(0, True, 0, length)
+
+
+            @pl.when((b > 0) & (b < blocks))
+            def _():
+                if p == 0:
+                    for which in range(3):
+                        load(which, b).wait()
+
+                    @pl.when(b + SLOTS - 1 < blocks)
+                    def _():
+                        start_load(b + SLOTS - 1, 0)
+
+                    elementwise(b, 0, length)
+                elif p == PIECE:
                     weight_grad(b, 0, NQ)
-                    input_grad(b, False)
+                elif p == 2 * PIECE:
+                    input_grad(b, False, 0, dot_rows * (length // dot_rows * 2 // 3))
+                elif p == 3 * PIECE:
+                    input_grad(b, False, dot_rows * (length // dot_rows * 2 // 3), length)
 
         @pl.when(h == done)
         def _():
@@ -489,23 +498,27 @@
                 small_to_left[...] = (small_from_right[...].astype(F32) + small[...]).astype(BF16)
                 small_left.start()
 
+        @pl.when(h == steps - 1 - (rep_count - 2))
+        def _():
+            small_out[...] = (
+                small_from_left[...].astype(F32) + small[...] + small_from_right[...].astype(F32)
+            )
+            for d in range(1, tp_count):
+                gather_copy(d, lax.rem(me + tp_count - d, tp_count)).wait_recv()
+            for d in range(1, tp_count):
+                gather_copy(d, me).wait_send()
+
+            @pl.when(has_right)
+            def _():
+                small_right.wait_send()
+
+            @pl.when(has_left)
+            def _():
+                small_left.wait_send()
+
         return carry
 
     lax.fori_loop(0, steps, step, 0)
-
-    small_out[...] = small_from_left[...].astype(F32) + small[...] + small_from_right[...].astype(F32)
-    for d in range(1, tp_count):
-        gather_copy(d, lax.rem(me + tp_count - d, tp_count)).wait_recv()
-    for d in range(1, tp_count):
-        gather_copy(d, me).wait_send()
-
-    @pl.when(has_right)
-    def _():
-        small_right.wait_send()
-
-    @pl.when(has_left)
-    def _():
-        small_left.wait_send()
 
 
 def spread(
@@ -625,7 +638,7 @@
             small_line,
             small_line,
             dma((3, SLOTS)),
-            dma((7,)),
+            dma((8,)),
             dma((WINDOW,)),
             dma((ring,)),
             dma((WINDOW,)),

time: 159 us -> 157 us (0.987)
  Pallas kernels: 159 us -> 156 us
    pallas_call x1, Pallas kernels: 153 us -> 151 us  [per_device(): pl.pallas_call(functools.partial(fused, rep_count, tp_count), out_shape=(...]
where the time goes in v3:
time: 157 us
  Pallas kernels  156 us (99%)
    pallas_call x1, Pallas kernels, per_device(): pl.pallas_call(functools.partial(fused, rep_count, tp_count), out_shape=(...  151 us
    pallas_call x1, Pallas kernels, per_device(): pl.pallas_call(spread, out_shape=(jax.ShapeDtypeStruct((length, width), B...  5.39 us

profile of v3, /device:TPU:0, one launch (start us, length us, event | category | flops | bytes accessed | tf_op | source)
XLA Modules:
  0.0 156.9 jit_solution(15355804702170494847)
XLA Ops:
  0.6 150.9 %shard_map.153 = (bf16[96,128,256]{2,1,0:T(8,128)(2,1)S(1)}, bf16[4,192,1024]{2,1,0:T(8,128)(2,1)S(1)}, f32[8,1536]{1,0:T(8,128)S(1)}) custom-call(bf16[768,1024]{1,0:T(8,128)(2,1)} %tokens.1, bf16[768,1536]{1,0:T(8,128)(2,1)} %gate_pre.1, bf16[768,1536]{1,0:T(8,128)(2,1)} %up_pre.1, bf16[768,1536]{1,0:T(8,128)(2,1)} %hidden.1, ...), custom_call_target="tpu_custom_call" | custom-call | tf_op jit(solution)/shard_map/pallas_call | solution.py:601
  151.5 5.4 %shard_map.154 = (bf16[768,1024]{1,0:T(8,128)(2,1)}, f32[1024,1536]{1,0:T(8,128)}, f32[1024,1536]{1,0:T(8,128)}, f32[3,1536]{1,0:T(4,128)}, f32[3,1536]{1,0:T(4,128)}, /*index=5*/f32[1536]{0:T(1024)}, f32[1536]{0:T(1024)}) custom-call(bf16[96,128,256]{2,1,0:T(8,128)(2,1)S(1)} %get-tuple-element.10.chunks_ref, ...), custom_call_target="tpu_custom_call" | custom-call | tf_op jit(solution)/shard_map/pallas_call | solution.py:668

commit v4 on v3

--- a/solution.py
+++ b/solution.py
@@ -9,12 +9,13 @@
 
 MESH = pl.DeviceIdType.MESH
 CW = 128
-NQ = 8
+NQ = 16
 PAD = 8
 TICKS = NQ // 2
 PIECE = TICKS // 4
-LAG = 3
-WINDOW = 3
+LAG_LEFT = 6
+LAG_RIGHT = 6
+WINDOW = 5
 SLOTS = 3
 TILE = 32
 F32 = jnp.float32
@@ -23,8 +24,8 @@
 
 def schedule(blocks, rep_count):
     done = blocks
-    last_tick = blocks * NQ + LAG * (rep_count - 1)
-    steps = max(-(-(last_tick - 1) // TICKS), done + 2 * rep_count, done + rep_count + 4)
+    last_tick = blocks * NQ + LAG_RIGHT * (rep_count - 1)
+    steps = max(-(-(last_tick - 1) // TICKS), done + 2 * rep_count, done + rep_count + 6)
     return done, steps
 
 
@@ -328,9 +329,9 @@
     term_rows = length // tp_count
 
     def move(tick):
-        c_right = tick - LAG * z
-        c_left = tick - LAG * (rep_count - 1 - z)
-        c_out = tick - LAG * (rep_count - 1)
+        c_right = tick - LAG_RIGHT * z
+        c_left = tick - LAG_LEFT * (rep_count - 1 - z)
+        c_out = jnp.minimum(c_right, c_left)
 
         @pl.when(has_left & (c_left >= WINDOW) & (c_left < chunks + WINDOW))
         def _():
@@ -432,6 +433,14 @@
         for p in range(TICKS):
             move(h * TICKS + p + 1)
 
+            @pl.when(h == done)
+            def _():
+                for k in range(p, tp_count, TICKS):
+                    term[k] = acc[k * term_rows : (k + 1) * term_rows, :].astype(BF16)
+                if p == TICKS - 1:
+                    for d in range(1, tp_count):
+                        scatter_copy(d).start()
+
             if p == TICKS // 2:
 
                 @pl.when(h == 0)
@@ -459,14 +468,7 @@
                 elif p == 3 * PIECE:
                     input_grad(b, False, dot_rows * (length // dot_rows * 2 // 3), length)
 
-        @pl.when(h == done)
-        def _():
-            for k in range(tp_count):
-                term[k] = acc[k * term_rows : (k + 1) * term_rows, :].astype(BF16)
-            for d in range(1, tp_count):
-                scatter_copy(d).start()
-
-        @pl.when(h == done + 4)
+        @pl.when(h == done + 5)
         def _():
             total = term[me].astype(F32)
             for d in range(1, tp_count):
@@ -590,7 +592,7 @@
     chunks = blocks * NQ
     rows_q = width // NQ
     term_rows = length // tp_count
-    ring = min(chunks, LAG * (rep_count - 1) + TICKS)
+    ring = min(chunks, LAG_RIGHT * (rep_count - 1) + TICKS)
     small_rows = 2 * taps + 2
     anywhere = pl.BlockSpec(memory_space=pl.ANY)
     vmem = pl.BlockSpec(memory_space=pltpu.VMEM)

time: 157 us -> 157 us (level)
  no operation moved by 1% of the time
where the time goes in v4:
time: 157 us
  Pallas kernels  156 us (99%)
    pallas_call x1, Pallas kernels, per_device(): pl.pallas_call(functools.partial(fused, rep_count, tp_count), out_shape=(...  151 us
    pallas_call x1, Pallas kernels, per_device(): pl.pallas_call(spread, out_shape=(jax.ShapeDtypeStruct((length, width), B...  5.43 us

profile of v4, /device:TPU:0, one launch (start us, length us, event | category | flops | bytes accessed | tf_op | source)
XLA Modules:
  0.0 157.0 jit_solution(15928776699792781494)
XLA Ops:
  0.6 150.9 %shard_map.153 = (bf16[192,64,256]{2,1,0:T(8,128)(2,1)S(1)}, bf16[4,192,1024]{2,1,0:T(8,128)(2,1)S(1)}, f32[8,1536]{1,0:T(8,128)S(1)}) custom-call(bf16[768,1024]{1,0:T(8,128)(2,1)} %tokens.1, bf16[768,1536]{1,0:T(8,128)(2,1)} %gate_pre.1, bf16[768,1536]{1,0:T(8,128)(2,1)} %up_pre.1, bf16[768,1536]{1,0:T(8,128)(2,1)} %hidden.1, ...), custom_call_target="tpu_custom_call" | custom-call | tf_op jit(solution)/shard_map/pallas_call | solution.py:603
  151.6 5.4 %shard_map.154 = (bf16[768,1024]{1,0:T(8,128)(2,1)}, f32[1024,1536]{1,0:T(8,128)}, f32[1024,1536]{1,0:T(8,128)}, f32[3,1536]{1,0:T(4,128)}, f32[3,1536]{1,0:T(4,128)}, /*index=5*/f32[1536]{0:T(1024)}, f32[1536]{0:T(1024)}) custom-call(bf16[192,64,256]{2,1,0:T(8,128)(2,1)S(1)} %get-tuple-element.10.chunks_ref, ...), custom_call_target="tpu_custom_call" | custom-call | tf_op jit(solution)/shard_map/pallas_call | solution.py:670
